TPU v7x, 256 devices: a whole 4x4x8 slice. The times are simulated.
256 devices in a mesh: sp: 64 (over z, y, core), tp: 4 (over x).
Axes of the slice: x: 4, y: 4, z: 8, core: 2. Of those that a mesh axis runs over, the one named last changes fastest.
Arguments:
- out_grad: bfloat16 [12288, 2048], P('sp'), may hold values from -16 to 16
- routes: int32 [12288, 2], P('sp'), may hold values from 0 to 63, all different within a row; in each aligned block of 192 rows (0 to 191, 192 to 383, ...) at most 12 rows name the same one
- route_weight: float32 [12288, 2], P('sp'), may hold values from 0.3 to 1.5
- expert_rows: bfloat16 [64, 64, 12, 2048], P(None, 'sp'), may hold values from -6 to 6
- gate_weight: bfloat16 [64, 2048, 1024], P('sp', None, 'tp'), may hold values from -0.125 to 0.125
- up_weight: bfloat16 [64, 2048, 1024], P('sp', None, 'tp'), may hold values from -0.125 to 0.125
- down_weight: bfloat16 [64, 1024, 2048], P('sp', 'tp'), may hold values from -0.1875 to 0.1875
- conv_input: bfloat16 [12288, 1024], P('sp', 'tp'), may hold values from -6 to 6
- out_gate: bfloat16 [12288, 1024], P('sp', 'tp'), may hold values from -6 to 6
- in_gate: bfloat16 [12288, 1024], P('sp', 'tp'), may hold values from -6 to 6
- taps: float32 [3, 1024], P(None, 'tp'), may hold values from -3 to 3
- out_weight: bfloat16 [2048, 1024], P(None, 'tp'), may hold values from -0.1875 to 0.1875
Outputs:
- gate_grad: bfloat16 [64, 2048, 1024], P('sp', None, 'tp')
- up_grad: bfloat16 [64, 2048, 1024], P('sp', None, 'tp')
- down_grad: bfloat16 [64, 1024, 2048], P('sp', 'tp')
- mid_grad: bfloat16 [12288, 2048], P('sp', 'tp')
- out_weight_grad: float32 [2048, 1024], P('sp', 'tp')
- input_grad: bfloat16 [12288, 1024], P('sp', 'tp')
- out_gate_grad: bfloat16 [12288, 1024], P('sp', 'tp')
- in_gate_grad: bfloat16 [12288, 1024], P('sp', 'tp')
Inputs may be any that keep to these rules, and one draw needn't show every extreme that they name: `routes`: each token names 2 different experts; within each aligned block of 192 tokens no expert is named by more than 12 tokens, a bound that some block reaches.
All inputs are finite; a program needn't handle non-finite values.
Results may differ from a plain program's by a relative error of at most 0.014.
Values may be sent and summed in bfloat16 or wider, within the bound.
No kernel may reach another device: no remote copies, remote signals or barrier semaphores. Data moves between devices by JAX's collectives and lax.ppermute only.
A program may use at most 64 MiB of HBM per device.

v0:
```python
import jax
import jax.numpy as jnp
from jax import lax
from jax.sharding import PartitionSpec as P


def split_up(shard, dim, peers):
    shape = shard.shape
    pieces = shard.reshape(*shape[:dim], peers, shape[dim] // peers, *shape[dim + 1 :])
    return jnp.moveaxis(pieces, dim, 0)


def sum_at_owner(shard, axis, dim):
    peers = lax.axis_size(axis)
    pieces = lax.all_to_all(split_up(shard, dim, peers), axis, 0, 0, tiled=True)
    return jnp.sum(pieces.astype(jnp.float32), axis=0)


def passed_along(shard, axis, by):
    peers = lax.axis_size(axis)
    pairs = [(i, i + by) for i in range(peers) if 0 <= i + by < peers]
    return lax.ppermute(shard, axis, pairs)


def on_device(
    out_grad,
    routes,
    route_weight,
    expert_rows,
    gate_weight,
    up_weight,
    down_weight,
    conv_input,
    out_gate,
    in_gate,
    taps,
    out_weight,
):
    groups = lax.axis_size("tp")
    member = lax.axis_index("tp")
    sources = lax.axis_size("sp")
    tok_rows, width = out_grad.shape
    top = routes.shape[1]
    local = gate_weight.shape[0]
    experts = local * sources
    slots = expert_rows.shape[2]
    share = width // groups
    flat = routes.reshape(-1)
    onehot = (flat[:, None] == jnp.arange(experts, dtype=jnp.int32)[None, :]).astype(jnp.int32)
    place = jnp.sum((jnp.cumsum(onehot, axis=0) - onehot) * onehot, axis=1)
    target = flat * slots + place
    slot_grad = (route_weight[:, :, None] * out_grad[:, None, :].astype(jnp.float32)).astype(
        jnp.bfloat16
    )
    outgoing = (
        jnp.zeros((experts * slots, width), jnp.bfloat16)
        .at[target]
        .set(slot_grad.reshape(-1, width))
    )
    outgoing = outgoing.reshape(sources, local, slots, width)
    portion = slots // groups
    piece = lax.dynamic_slice_in_dim(outgoing, member * portion, portion, 2)
    arrived = lax.all_to_all(piece, "sp", split_axis=0, concat_axis=0, tiled=True)
    grads = lax.all_gather(arrived, "tp", axis=2, tiled=True)
    gate = jnp.einsum(
        "secd,edf->secf", expert_rows, gate_weight, preferred_element_type=jnp.float32
    )
    up = jnp.einsum("secd,edf->secf", expert_rows, up_weight, preferred_element_type=jnp.float32)
    sig = jax.nn.sigmoid(gate)
    act = (gate * sig * up).astype(jnp.bfloat16)
    act_grad = jnp.einsum("secd,efd->secf", grads, down_weight, preferred_element_type=jnp.float32)
    up_part = (act_grad * gate * sig).astype(jnp.bfloat16)
    gate_part = (act_grad * up * sig * (1.0 + gate * (1.0 - sig))).astype(jnp.bfloat16)
    down_grad = jnp.einsum("secf,secd->efd", act, grads, preferred_element_type=jnp.float32).astype(
        jnp.bfloat16
    )
    gate_grad = jnp.einsum(
        "secd,secf->edf", expert_rows, gate_part, preferred_element_type=jnp.float32
    ).astype(jnp.bfloat16)
    up_grad = jnp.einsum(
        "secd,secf->edf", expert_rows, up_part, preferred_element_type=jnp.float32
    ).astype(jnp.bfloat16)
    row_part = jnp.einsum(
        "secf,edf->secd", gate_part, gate_weight, preferred_element_type=jnp.float32
    )
    row_part = row_part + jnp.einsum(
        "secf,edf->secd", up_part, up_weight, preferred_element_type=jnp.float32
    )
    summed = sum_at_owner(row_part.astype(jnp.bfloat16), "tp", 3)
    returned = lax.all_to_all(
        summed.astype(jnp.bfloat16), "sp", split_axis=0, concat_axis=0, tiled=True
    )
    returned = returned.reshape(experts * slots, share)
    picked = (
        jnp.take(returned, target, axis=0)
        .astype(jnp.float32)
        .reshape(tok_rows, top, share)
        .sum(axis=1)
    )
    own_cols = lax.dynamic_slice_in_dim(out_grad, member * share, share, 1).astype(jnp.float32)
    mid_grad = (own_cols + picked).astype(jnp.bfloat16)
    mid_whole = lax.all_gather(mid_grad, "tp", axis=1, tiled=True)
    reach = taps.shape[0] - 1
    rims = jnp.stack([in_gate[tok_rows - reach :], conv_input[tok_rows - reach :]])
    prior = passed_along(rims, "sp", 1)
    mixed = in_gate.astype(jnp.float32) * conv_input.astype(jnp.float32)
    prior_mixed = prior[0].astype(jnp.float32) * prior[1].astype(jnp.float32)
    extended = jnp.concatenate([prior_mixed, mixed], axis=0)
    conv = jnp.zeros_like(mixed)
    for tap in range(reach + 1):
        conv = conv + taps[tap][None, :] * extended[reach - tap : reach - tap + tok_rows]
    gated = (out_gate.astype(jnp.float32) * conv).astype(jnp.bfloat16)
    out_weight_grad = sum_at_owner(
        lax.dot_general(
            mid_whole, gated, (((0,), (0,)), ((), ())), preferred_element_type=jnp.float32
        ).astype(jnp.bfloat16),
        "sp",
        0,
    )
    gated_grad = jnp.dot(mid_whole, out_weight, preferred_element_type=jnp.float32)
    out_gate_grad = (gated_grad * conv).astype(jnp.bfloat16)
    conv_grad = gated_grad * out_gate.astype(jnp.float32)
    later = passed_along(conv_grad[:reach], "sp", -1)
    following = jnp.concatenate([conv_grad, later], axis=0)
    mixed_grad = jnp.zeros_like(conv_grad)
    for tap in range(reach + 1):
        mixed_grad = mixed_grad + taps[tap][None, :] * following[tap : tap + tok_rows]
    input_grad = (mixed_grad * in_gate.astype(jnp.float32)).astype(jnp.bfloat16)
    in_gate_grad = (mixed_grad * conv_input.astype(jnp.float32)).astype(jnp.bfloat16)
    return (
        gate_grad,
        up_grad,
        down_grad,
        mid_grad,
        out_weight_grad,
        input_grad,
        out_gate_grad,
        in_gate_grad,
    )


def solution(mesh):
    in_specs = (
        P("sp", None),
        P("sp", None),
        P("sp", None),
        P(None, "sp", None, None),
        P("sp", None, "tp"),
        P("sp", None, "tp"),
        P("sp", "tp", None),
        P("sp", "tp"),
        P("sp", "tp"),
        P("sp", "tp"),
        P(None, "tp"),
        P(None, "tp"),
    )
    out_specs = (
        P("sp", None, "tp"),
        P("sp", None, "tp"),
        P("sp", "tp", None),
        P("sp", "tp"),
        P("sp", "tp"),
        P("sp", "tp"),
        P("sp", "tp"),
        P("sp", "tp"),
    )
    return jax.shard_map(
        on_device, mesh=mesh, in_specs=in_specs, out_specs=out_specs, check_vma=False
    )
```

profile of v0, /device:TPU:1, one launch (start us, length us, event | category | flops | bytes accessed | tf_op | source)
XLA Modules:
  0.0 281.8 jit_solution(15357142444350941405)
XLA Ops:
  10.7 4.4 %mul.148 = f32[192,2,2048]{2,1,0:T(2,128)} broadcast(bf16[192,2048]{1,0:T(8,128)(2,1)} %param.12), dimensions={0,2} | broadcast | bytes 3932160 | tf_op jit(solution)/shard_map/mul | solution.py:52
  15.1 5.3 %mul.149 = f32[384,2048]{1,0:T(8,128)} reshape(f32[192,2,2048]{2,1,0:T(2,128)} %mul.148) | data formatting | bytes 6291456 | tf_op jit(solution)/shard_map/mul | solution.py:52
  20.8 6.4 %scatter_custom_fusion = bf16[768,2048]{1,0:T(8,128)(2,1)} fusion(s32[384]{0:T(512)S(1)} %fusion.80, f32[384,2048]{1,0:T(8,128)} %mul.149, f32[384]{0:T(512)S(1)} %mul.146, bf16[]{:T(256)} %constant.12.clone.1), kind=kCustom, calls=%fused_computation.28 | custom fusion | flops 1572864 | bytes 6293506 | tf_op jit(solution)/shard_map/scatter | solution.py:58
  27.2 6.1 %reshape.145 = bf16[64,1,12,2048]{3,2,0,1:T(8,128)(2,1)} reshape(bf16[768,2048]{1,0:T(8,128)(2,1)} %scatter_custom_fusion) | data formatting | bytes 6291456 | tf_op jit(solution)/shard_map/reshape | solution.py:60
  33.2 3.0 %dynamic-slice_bitcast_fusion = bf16[64,1,3,2048]{3,2,1,0:T(4,128)(2,1)S(1)} fusion(bf16[64,1,12,2048]{3,2,0,1:T(8,128)(2,1)} %reshape.145, s32[]{:T(128)S(6)} %select_n.30), kind=kLoop, calls=%fused_computation.40 | loop fusion | bytes 1572868 | tf_op jit(solution)/shard_map/dynamic_slice | solution.py:62
  36.3 41.1 %all_to_all.20 = bf16[64,1,3,2048]{3,2,1,0:T(4,128)(2,1)S(1)} all-to-all(bf16[64,1,3,2048]{3,2,1,0:T(4,128)(2,1)S(1)} %dynamic-slice_bitcast_fusion), channel_id=1, replica_groups=mesh['sp'=64,'tp'=4] {'sp'}, dimensions={0} | all-to-all | bytes 1572864 | tf_op jit(solution)/shard_map/all_to_all | solution.py:63
  78.9 3.2 %fusion.48 = f32[64,1,12,256]{3,0,2,1:T(8,128)} fusion(bf16[64,1,12,2048]{3,0,2,1:T(8,128)(2,1)S(1)} %copy-done, bf16[1,2048,256]{2,1,0:T(8,128)(2,1)} %param.16), kind=kOutput, calls=%fused_computation.33 | convolution fusion | flops 805306368 | bytes 4980736 | tf_op jit(solution)/shard_map/secd,edf->secf/dot_general | solution.py:65
  84.0 33.8 %all-gather.2.cloned.1.call-done = bf16[64,1,12,2048]{3,0,1,2:T(8,128)(2,1)} async-done(((bf16[64,1,3,2048]{3,0,1,2:T(8,128)(2,1)}), bf16[64,1,12,2048]{3,0,1,2:T(8,128)(2,1)}) %all-gather.2.cloned.1.call-update) | async-done | bytes 3145744 | tf_op jit(solution)/shard_map/all_gather | solution.py:64
  117.8 3.9 %multiply_convert_fusion.3 = (bf16[64,1,12,256]{3,0,2,1:T(8,128)(2,1)S(1)}, bf16[64,1,12,256]{3,0,2,1:T(8,128)(2,1)S(1)}) fusion(f32[64,1,12,256]{3,0,2,1:T(8,128)} %fusion.48, f32[64,1,12,256]{3,0,2,1:T(8,128)} %fusion.45, bf16[1,256,2048]{2,1,0:T(8,128)(2,1)} %param.18, bf16[64,1,12,2048]{3,0,1,2:T(8,128)(2,1)} %all-gather.2.cloned.1.call-done), kind=kOutput, calls=%fused_computation.43 | convolution fusion | flops 807862272 | bytes 6553600 | tf_op jit(solution)/shard_map/secd,efd->secf/dot_general | solution.py:71
  124.6 39.9 %all_to_all.21 = bf16[4,64,1,12,512]{4,1,3,2,0:T(8,128)(2,1)} all-to-all(bf16[4,64,1,12,512]{4,1,3,2,0:T(8,128)(2,1)S(1)} %bitcast.161), channel_id=1, replica_groups=mesh['sp'=64,'tp'=4] {'tp'}, dimensions={0} | all-to-all | bytes 6291456 | tf_op jit(solution)/shard_map/all_to_all | solution.py:15
  164.5 3.5 %reduce_sum.48 = bf16[64,12,512]{2,0,1:T(8,128)(2,1)} reduce(bf16[4,64,1,12,512]{4,1,3,2,0:T(8,128)(2,1)} %all_to_all.21, bf16[]{:T(256)} %constant.12.clone.1), dimensions={0,2}, to_apply=%region_4.5 | reduce | flops 1179648 | bytes 3932162 | tf_op jit(solution)/shard_map/reduce_sum | solution.py:16
  168.1 2.5 copy.54
  170.6 12.1 %all-to-all-start.2 = ((bf16[64,1,12,512]{3,2,1,0:T(8,128)(2,1)}), bf16[64,1,12,512]{3,2,1,0:T(8,128)(2,1)}, u32[]{:S(2)}, u32[]{:S(2)}) async-start(bf16[64,1,12,512]{3,2,1,0:T(8,128)(2,1)} %copy.54), calls=%async_computation.2 | async-start | bytes 2097152 | tf_op jit(solution)/shard_map/all_to_all | solution.py:90
  182.8 3.5 %collective-permute-start = (bf16[2,2,256]{2,1,0:T(2,128)(2,1)S(1)}, bf16[2,2,256]{2,1,0:T(2,128)(2,1)S(1)}, u32[]{:S(2)}, u32[]{:S(2)}) collective-permute-start(bf16[2,2,256]{2,1,0:T(2,128)(2,1)S(1)} %pad_maximum_fusion.2), channel_id=1, source_target_pairs={{0,4},{4,8},{8,12},{12,16},{16,20},{20,24},{24,28},{28,32},{32,36}... | collective-permute-start | bytes 6152 | tf_op jit(solution)/shard_map/ppermute | solution.py:22
  188.6 22.2 %all-to-all-done.2 = bf16[64,1,12,512]{3,2,1,0:T(8,128)(2,1)} async-done(((bf16[64,1,12,512]{3,2,1,0:T(8,128)(2,1)}), bf16[64,1,12,512]{3,2,1,0:T(8,128)(2,1)}, u32[]{:S(2)}, u32[]{:S(2)}) %all-to-all-start.2) | async-done | bytes 786464 | tf_op jit(solution)/shard_map/all_to_all | solution.py:90
  212.9 3.3 %gather_fusion = bf16[384,512]{1,0:T(8,128)(2,1)S(1)} fusion(bf16[768,512]{1,0:T(8,128)(2,1)} %reshape.155, s32[1024]{0:T(1024)S(1)} %pad_clamp_fusion), kind=kCustom, calls=%fused_computation | custom fusion | bytes 787968 | tf_op jit(solution)/shard_map/jit(_take)/gather | solution.py:95
  220.3 11.0 %all_gather.7 = bf16[192,2048]{1,0:T(8,128)(2,1)S(1)} all-gather(bf16[192,512]{1,0:T(8,128)(2,1)S(1)} %add_convert_fusion.1), channel_id=1, replica_groups=mesh['sp'=64,'tp'=4] {'tp'}, dimensions={1}, use_global_device_ids=true | all-gather | bytes 983040 | tf_op jit(solution)/shard_map/all_gather | solution.py:102
  231.3 2.5 multiply_convert_fusion.6
  235.2 9.6 %all-to-all-start.3 = ((bf16[64,32,256]{2,1,0:T(8,128)(2,1)}), bf16[64,32,256]{2,1,0:T(8,128)(2,1)}, u32[]{:S(2)}, u32[]{:S(2)}) async-start(bf16[64,32,256]{2,1,0:T(8,128)(2,1)} %bitcast.163), calls=%async_computation.3 | async-start | bytes 2097152 | tf_op jit(solution)/shard_map/all_to_all | solution.py:15
  244.9 3.1 %fusion.33 = bf16[1,2048,256]{1,2,0:T(8,128)(2,1)} fusion(bf16[64,1,12,2048]{3,0,2,1:T(8,128)(2,1)S(1)} %copy-done, bf16[64,1,12,256]{3,0,2,1:T(8,128)(2,1)} %copy-done.12), kind=kOutput, calls=%fused_computation.25 | convolution fusion | flops 805830656 | bytes 4587520 | tf_op jit(solution)/shard_map/secd,secf->edf/dot_general | solution.py:77
  250.6 2.4 collective-permute-start.1
  255.1 2.3 copy.55
  257.4 2.3 copy.56
  261.0 11.9 %all-to-all-done.3 = bf16[64,32,256]{2,1,0:T(8,128)(2,1)} async-done(((bf16[64,32,256]{2,1,0:T(8,128)(2,1)}), bf16[64,32,256]{2,1,0:T(8,128)(2,1)}, u32[]{:S(2)}, u32[]{:S(2)}) %all-to-all-start.3) | async-done | bytes 1048608 | tf_op jit(solution)/shard_map/all_to_all | solution.py:15
  (84 shorter events, 28.0 us)
Async XLA Ops:
  7.2 71.7 %copy-start = (bf16[64,1,12,2048]{3,0,2,1:T(8,128)(2,1)S(1)}, bf16[64,1,12,2048]{3,0,2,1:T(8,128)(2,1)}, u32[]{:S(2)}) copy-start(bf16[64,1,12,2048]{3,0,2,1:T(8,128)(2,1)} %param.15) | copy-start | bytes 9437188
  7.2 110.6 %all-gather.2.cloned.1.call-start = ((), (), s32[]{:S(2)}) async-start(), calls=%async_computation.4 | async-start | bytes 3932160 | tf_op jit(solution)/shard_map/all_gather | solution.py:64
  15.1 5.3 %copy-start.16 = (f32[192,2]{0,1:T(2,128)S(1)}, f32[192,2]{0,1:T(2,128)}, u32[]{:S(2)}) copy-start(f32[192,2]{0,1:T(2,128)} %param.14) | copy-start | bytes 4612
  78.9 3.2 %copy-start.2 = (bf16[1,2048,256]{2,1,0:T(8,128)(2,1)S(1)}, bf16[1,2048,256]{2,1,0:T(8,128)(2,1)}, u32[]{:S(2)}) copy-start(bf16[1,2048,256]{2,1,0:T(8,128)(2,1)} %param.17) | copy-start | bytes 3145732
  117.8 3.9 %copy-start.1 = (bf16[1,2048,256]{2,1,0:T(8,128)(2,1)S(1)}, bf16[1,2048,256]{2,1,0:T(8,128)(2,1)}, u32[]{:S(2)}) copy-start(bf16[1,2048,256]{2,1,0:T(8,128)(2,1)} %param.16) | copy-start | bytes 3145732
  121.7 1.1 copy-start.12
  121.7 1.5 copy-start.3
  164.5 18.2 %copy-start.5 = (bf16[192,256]{1,0:T(8,128)(2,1)S(1)}, bf16[192,256]{1,0:T(8,128)(2,1)}, u32[]{:S(2)}) copy-start(bf16[192,256]{1,0:T(8,128)(2,1)} %param.19) | copy-start | bytes 294916
  164.5 18.2 %copy-start.7 = (bf16[192,256]{1,0:T(8,128)(2,1)S(1)}, bf16[192,256]{1,0:T(8,128)(2,1)}, u32[]{:S(2)}) copy-start(bf16[192,256]{1,0:T(8,128)(2,1)} %param.21) | copy-start | bytes 294916
  164.5 22.0 %copy-start.13 = (s32[192,2]{0,1:T(2,128)S(1)}, s32[192,2]{0,1:T(2,128)}, u32[]{:S(2)}) copy-start(s32[192,2]{0,1:T(2,128)} %param.13) | copy-start | bytes 4612
  164.5 22.1 %copy-start.15 = (f32[3,256]{1,0:T(4,128)S(1)}, f32[3,256]{1,0:T(4,128)}, u32[]{:S(2)}) copy-start(f32[3,256]{1,0:T(4,128)} %param.22) | copy-start | bytes 9220
  170.6 40.2 %all-to-all-start.2 = ((bf16[64,1,12,512]{3,2,1,0:T(8,128)(2,1)}), bf16[64,1,12,512]{3,2,1,0:T(8,128)(2,1)}, u32[]{:S(2)}, u32[]{:S(2)}) async-start(bf16[64,1,12,512]{3,2,1,0:T(8,128)(2,1)} %copy.54), calls=%async_computation.2 | async-start | bytes 2097152 | tf_op jit(solution)/shard_map/all_to_all | solution.py:90
  182.8 5.3 %collective-permute-start = (bf16[2,2,256]{2,1,0:T(2,128)(2,1)S(1)}, bf16[2,2,256]{2,1,0:T(2,128)(2,1)S(1)}, u32[]{:S(2)}, u32[]{:S(2)}) collective-permute-start(bf16[2,2,256]{2,1,0:T(2,128)(2,1)S(1)} %pad_maximum_fusion.2), channel_id=1, source_target_pairs={{0,4},{4,8},{8,12},{12,16},{16,20},{20,24},{24,28},{28,32},{32,36}... | collective-permute-start | bytes 6152 | tf_op jit(solution)/shard_map/ppermute | solution.py:22
  216.2 15.1 %copy-start.14 = (f32[2,256]{1,0:T(2,128)S(1)}, f32[2,256]{1,0:T(2,128)}, u32[]{:S(2)}) copy-start(f32[2,256]{1,0:T(2,128)} %multiply_bitcast_fusion) | copy-start | bytes 6148
  217.1 16.6 %copy-start.9 = (bf16[192,256]{1,0:T(8,128)(2,1)S(1)}, bf16[192,256]{1,0:T(8,128)(2,1)}, u32[]{:S(2)}) copy-start(bf16[192,256]{1,0:T(8,128)(2,1)} %param.20) | copy-start | bytes 294916
  220.3 14.9 %copy-start.4 = (bf16[192,512]{1,0:T(8,128)(2,1)}, bf16[192,512]{1,0:T(8,128)(2,1)S(1)}, u32[]{:S(2)}) copy-start(bf16[192,512]{1,0:T(8,128)(2,1)S(1)} %add_convert_fusion.1) | copy-start | bytes 589828
  235.2 37.7 %all-to-all-start.3 = ((bf16[64,32,256]{2,1,0:T(8,128)(2,1)}), bf16[64,32,256]{2,1,0:T(8,128)(2,1)}, u32[]{:S(2)}, u32[]{:S(2)}) async-start(bf16[64,32,256]{2,1,0:T(8,128)(2,1)} %bitcast.163), calls=%async_computation.3 | async-start | bytes 2097152 | tf_op jit(solution)/shard_map/all_to_all | solution.py:15
  244.9 3.2 %copy-start.17 = (bf16[64,1,12,2048]{3,0,1,2:T(8,128)(2,1)S(1)}, bf16[64,1,12,2048]{3,0,1,2:T(8,128)(2,1)}, u32[]{:S(2)}) copy-start(bf16[64,1,12,2048]{3,0,1,2:T(8,128)(2,1)} %all-gather.2.cloned.1.call-done) | copy-start | bytes 9437188
  244.9 3.1 %copy-start.18 = (f32[64,1,12,256]{3,0,2,1:T(8,128)S(1)}, f32[64,1,12,256]{3,0,2,1:T(8,128)}, u32[]{:S(2)}) copy-start(f32[64,1,12,256]{3,0,2,1:T(8,128)} %fusion.48) | copy-start | bytes 2359300
  244.9 3.1 %copy-start.19 = (f32[64,1,12,256]{3,0,2,1:T(8,128)S(1)}, f32[64,1,12,256]{3,0,2,1:T(8,128)}, u32[]{:S(2)}) copy-start(f32[64,1,12,256]{3,0,2,1:T(8,128)} %fusion.45) | copy-start | bytes 2359300
  248.0 5.1 %copy-start.11 = (bf16[64,1,12,256]{3,0,2,1:T(8,128)(2,1)S(1)}, bf16[64,1,12,256]{3,0,2,1:T(8,128)(2,1)}, u32[]{:S(2)}) copy-start(bf16[64,1,12,256]{3,0,2,1:T(8,128)(2,1)} %copy-done.10) | copy-start | bytes 1179652
  250.6 9.0 %collective-permute-start.1 = (f32[2,256]{1,0:T(2,128)}, f32[2,256]{1,0:T(2,128)S(1)}, u32[]{:S(2)}, u32[]{:S(2)}) collective-permute-start(f32[2,256]{1,0:T(2,128)} %slice.66), channel_id=1, source_target_pairs={{4,0},{8,4},{12,8},{16,12},{20,16},{24,20},{28,24},{32,28},{36,32}... | collective-permute-start | bytes 6152 | tf_op jit(solution)/shard_map/ppermute | solution.py:22
  255.1 4.6 %copy-start.6 = (bf16[192,256]{1,0:T(8,128)(2,1)S(1)}, bf16[192,256]{1,0:T(8,128)(2,1)}, u32[]{:S(2)}) copy-start(bf16[192,256]{1,0:T(8,128)(2,1)} %param.19) | copy-start | bytes 294916
  255.1 5.3 %copy-start.8 = (bf16[192,256]{1,0:T(8,128)(2,1)S(1)}, bf16[192,256]{1,0:T(8,128)(2,1)}, u32[]{:S(2)}) copy-start(bf16[192,256]{1,0:T(8,128)(2,1)} %param.21) | copy-start | bytes 294916
  (1 other events, 1.1 us)
Sparse Core Ops, SparseCore 0:
  79.0 38.7 all-gather.1
where the time goes:
time: 283 us; the launch traced here: 282 us
  blocking collectives  92 us (33%)
  waiting for transfers between devices  67.9 us (24%)
  local copies, waits for them, and re-layouts  37.9 us (13%)
  starting transfers between devices  27.8 us (10%)
  matrix products  22 us (8%)
  other arithmetic  19.7 us (7%)
  between operations  14.4 us (5%)
    all_to_all x1, blocking collectives, on_device(): lax.all_to_all(piece, 'sp', split_axis=0, concat_axis=0, tiled=True)  41.1 us
    all_to_all x1, blocking collectives, sum_at_owner(): pieces = lax.all_to_all(split_up(shard, dim, peers), axis, 0, 0, tiled=True)  39.9 us
    all_gather x1, waiting for transfers between devices, on_device(): grads = lax.all_gather(arrived, 'tp', axis=2, tiled=True)  33.8 us
    all_to_all x1, waiting for transfers between devices, on_device(): lax.all_to_all(summed.astype(jnp.bfloat16), 'sp', split_axis=0, concat_ax...  22.2 us
    all_to_all x1, starting transfers between devices, on_device(): lax.all_to_all(summed.astype(jnp.bfloat16), 'sp', split_axis=0, concat_ax...  12.1 us
    all_to_all x1, waiting for transfers between devices, sum_at_owner(): pieces = lax.all_to_all(split_up(shard, dim, peers), axis, 0, 0, tiled=True)  11.9 us
    all_gather x1, blocking collectives, on_device(): mid_whole = lax.all_gather(mid_grad, 'tp', axis=1, tiled=True)  11 us
    mul x3, local copies, waits for them, and re-layouts, on_device(): route_weight[:, :, None] * out_grad[:, None, :].astype(jnp.float32)  9.84 us
  transfers between devices with their start and end apart: 5, of which 3 were waited for; matrix products, arithmetic and copies ran while one was open for 7% of the time, Pallas kernels for 0%

commit v1 on v0

--- a/solution.py
+++ b/solution.py
@@ -2,6 +2,27 @@
 import jax.numpy as jnp
 from jax import lax
 from jax.sharding import PartitionSpec as P
+
+
+def gather_around(shard, axis, dim):
+    size, index, rows = (lax.axis_size(axis), lax.axis_index(axis), shard.shape[dim])
+    right = [(i, (i + 1) % size) for i in range(size)]
+    downward = [(i, (i - 1) % size) for i in range(size)]
+    out = jnp.zeros((*shard.shape[:dim], size * rows, *shard.shape[dim + 1 :]), shard.dtype)
+    out = lax.dynamic_update_slice_in_dim(out, shard, index * rows, axis=dim)
+    from_left = from_right = shard
+    half = size // 2
+    for step in range(1, half + 1):
+        from_left = lax.ppermute(from_left, axis, right)
+        out = lax.dynamic_update_slice_in_dim(
+            out, from_left, (index - step) % size * rows, axis=dim
+        )
+        if step < size - half:
+            from_right = lax.ppermute(from_right, axis, downward)
+            out = lax.dynamic_update_slice_in_dim(
+                out, from_right, (index + step) % size * rows, axis=dim
+            )
+    return out
 
 
 def split_up(shard, dim, peers):
@@ -61,7 +82,7 @@
     portion = slots // groups
     piece = lax.dynamic_slice_in_dim(outgoing, member * portion, portion, 2)
     arrived = lax.all_to_all(piece, "sp", split_axis=0, concat_axis=0, tiled=True)
-    grads = lax.all_gather(arrived, "tp", axis=2, tiled=True)
+    grads = gather_around(arrived, "tp", 2)
     gate = jnp.einsum(
         "secd,edf->secf", expert_rows, gate_weight, preferred_element_type=jnp.float32
     )

time: 283 us -> 265 us (0.936)
  blocking collectives: 92 us -> 48.8 us
  waiting for transfers between devices: 67.9 us -> 88.8 us
  starting transfers between devices: 27.8 us -> 43.5 us
  between operations: 14.4 us -> 1.12 us
  local copies, waits for them, and re-layouts: 37.9 us -> 42.4 us
    all_to_all x1 -> x0, blocking collectives: 41.1 us -> none  [on_device(): lax.all_to_all(piece, 'sp', split_axis=0, concat_axis=0, tiled=True)]
    all_gather x1 -> x0, waiting for transfers between devices: 33.8 us -> none  [on_device(): grads = lax.all_gather(arrived, 'tp', axis=2, tiled=True)]
    ppermute x0 -> x3, waiting for transfers between devices: none -> 29.8 us  [the longest x2 27.6 us: gather_around(): from_left = lax.ppermute(from_left, axis, right)]
    all_to_all x0 -> x1, waiting for transfers between devices: none -> 24.9 us  [on_device(): lax.all_to_all(piece, 'sp', split_axis=0, concat_axis=0, tiled=True)]
    all_to_all x0 -> x1, starting transfers between devices: none -> 13.3 us  [on_device(): lax.all_to_all(piece, 'sp', split_axis=0, concat_axis=0, tiled=True)]
    ppermute x0 -> x3, starting transfers between devices: none -> 3.01 us  [the longest x1 1.72 us: gather_around(): from_right = lax.ppermute(from_right, axis, downward)]
    unnamed x44 -> x50, local copies, waits for them, and re-layouts: 6.07 us -> 6.65 us
  transfers between devices with their start and end apart: 5 -> 8, of which waited for: 3 -> 6; matrix products, arithmetic and copies ran while one was open for 7% -> 9% of each run, Pallas kernels for 0% -> 0%
where the time goes in v1:
time: 265 us; the launch traced here: 264 us
  waiting for transfers between devices  88.8 us (34%)
  blocking collectives  48.8 us (18%)
  starting transfers between devices  43.5 us (16%)
  local copies, waits for them, and re-layouts  42.4 us (16%)
  other arithmetic  19.8 us (7%)
  matrix products  19.6 us (7%)
    all_to_all x1, blocking collectives, sum_at_owner(): pieces = lax.all_to_all(split_up(shard, dim, peers), axis, 0, 0, tiled=True)  37.9 us
    ppermute x2, waiting for transfers between devices, gather_around(): from_left = lax.ppermute(from_left, axis, right)  27.6 us
    all_to_all x1, waiting for transfers between devices, on_device(): lax.all_to_all(piece, 'sp', split_axis=0, concat_axis=0, tiled=True)  24.9 us
    all_to_all x1, waiting for transfers between devices, on_device(): lax.all_to_all(summed.astype(jnp.bfloat16), 'sp', split_axis=0, concat_ax...  22.2 us
    all_to_all x1, starting transfers between devices, on_device(): lax.all_to_all(piece, 'sp', split_axis=0, concat_axis=0, tiled=True)  13.3 us
    all_to_all x1, waiting for transfers between devices, sum_at_owner(): pieces = lax.all_to_all(split_up(shard, dim, peers), axis, 0, 0, tiled=True)  11.9 us
    all_to_all x1, starting transfers between devices, on_device(): lax.all_to_all(summed.astype(jnp.bfloat16), 'sp', split_axis=0, concat_ax...  11.5 us
    all_gather x1, blocking collectives, on_device(): mid_whole = lax.all_gather(mid_grad, 'tp', axis=1, tiled=True)  11 us
  transfers between devices with their start and end apart: 8, of which 6 were waited for; matrix products, arithmetic and copies ran while one was open for 9% of the time, Pallas kernels for 0%

profile of v1, /device:TPU:1, one launch (start us, length us, event | category | flops | bytes accessed | tf_op | source)
XLA Modules:
  0.0 263.9 jit_solution(18041572222220663740)
XLA Ops:
  4.2 4.4 %mul.158 = f32[192,2,2048]{2,1,0:T(2,128)} broadcast(bf16[192,2048]{1,0:T(8,128)(2,1)} %param.12), dimensions={0,2} | broadcast | bytes 3932160 | tf_op jit(solution)/shard_map/mul | solution.py:73
  8.6 5.3 %mul.159 = f32[384,2048]{1,0:T(8,128)} reshape(f32[192,2,2048]{2,1,0:T(2,128)} %mul.158) | data formatting | bytes 6291456 | tf_op jit(solution)/shard_map/mul | solution.py:73
  14.2 6.4 %scatter_custom_fusion = bf16[768,2048]{1,0:T(8,128)(2,1)} fusion(s32[384]{0:T(512)S(1)} %fusion.66, f32[384,2048]{1,0:T(8,128)} %mul.159, f32[384]{0:T(512)S(1)} %mul.156, bf16[]{:T(256)} %constant.58.clone.1), kind=kCustom, calls=%fused_computation.24 | custom fusion | flops 1572864 | bytes 6293506 | tf_op jit(solution)/shard_map/scatter | solution.py:79
  20.6 6.0 %reshape.159 = bf16[64,1,12,2048]{3,2,0,1:T(8,128)(2,1)} reshape(bf16[768,2048]{1,0:T(8,128)(2,1)} %scatter_custom_fusion) | data formatting | bytes 6291456 | tf_op jit(solution)/shard_map/reshape | solution.py:81
  26.7 4.0 %dynamic-slice_bitcast_fusion = bf16[64,1,3,2048]{3,2,1,0:T(4,128)(2,1)} fusion(bf16[64,1,12,2048]{3,2,0,1:T(8,128)(2,1)} %reshape.159, s32[]{:T(128)S(6)} %select_n.55), kind=kLoop, calls=%fused_computation.36 | loop fusion | bytes 1572868 | tf_op jit(solution)/shard_map/dynamic_slice | solution.py:83
  30.7 13.3 %all-to-all-start = ((bf16[64,1,3,2048]{3,2,1,0:T(4,128)(2,1)}), bf16[64,1,3,2048]{3,2,1,0:T(4,128)(2,1)}, u32[]{:S(2)}, u32[]{:S(2)}) async-start(bf16[64,1,3,2048]{3,2,1,0:T(4,128)(2,1)} %dynamic-slice_bitcast_fusion), calls=%async_computation | async-start | bytes 2097152 | tf_op jit(solution)/shard_map/all_to_all | solution.py:84
  44.1 3.1 %fusion.34 = f32[64,1,12,256]{3,0,2,1:T(8,128)} fusion(bf16[64,1,12,2048]{3,0,2,1:T(8,128)(2,1)S(1)} %copy-done, bf16[1,2048,256]{2,1,0:T(8,128)(2,1)} %param.16), kind=kOutput, calls=%fused_computation.28 | convolution fusion | flops 805306368 | bytes 4980736 | tf_op jit(solution)/shard_map/secd,edf->secf/dot_general | solution.py:86
  47.2 24.9 %all-to-all-done = bf16[64,1,3,2048]{3,2,1,0:T(4,128)(2,1)} async-done(((bf16[64,1,3,2048]{3,2,1,0:T(4,128)(2,1)}), bf16[64,1,3,2048]{3,2,1,0:T(4,128)(2,1)}, u32[]{:S(2)}, u32[]{:S(2)}) %all-to-all-start) | async-done | bytes 786464 | tf_op jit(solution)/shard_map/all_to_all | solution.py:84
  81.5 11.6 %collective-permute-done = bf16[64,1,3,2048]{3,0,2,1:T(8,128)(2,1)S(1)} collective-permute-done((bf16[64,1,3,2048]{3,0,2,1:T(8,128)(2,1)S(1)}, bf16[64,1,3,2048]{3,0,2,1:T(8,128)(2,1)S(1)}, u32[]{:S(2)}, u32[]{:S(2)}) %collective-permute-start) | collective-permute-done | bytes 786464 | tf_op jit(solution)/shard_map/ppermute | solution.py:16
  95.4 16.0 %collective-permute-done.2 = bf16[64,1,3,2048]{3,0,2,1:T(8,128)(2,1)S(1)} collective-permute-done((bf16[64,1,3,2048]{3,0,2,1:T(8,128)(2,1)S(1)}, bf16[64,1,3,2048]{3,0,2,1:T(8,128)(2,1)S(1)}, u32[]{:S(2)}, u32[]{:S(2)}) %collective-permute-start.2) | collective-permute-done | bytes 786464 | tf_op jit(solution)/shard_map/ppermute | solution.py:16
  116.2 37.9 %all_to_all.20 = bf16[4,64,1,12,512]{4,1,3,2,0:T(8,128)(2,1)} all-to-all(bf16[4,64,1,12,512]{4,1,3,2,0:T(8,128)(2,1)S(1)} %bitcast.155), channel_id=1, replica_groups=mesh['sp'=64,'tp'=4] {'tp'}, dimensions={0} | all-to-all | bytes 6291456 | tf_op jit(solution)/shard_map/all_to_all | solution.py:36
  154.1 3.5 %reduce_sum.48 = bf16[64,12,512]{2,0,1:T(8,128)(2,1)} reduce(bf16[4,64,1,12,512]{4,1,3,2,0:T(8,128)(2,1)} %all_to_all.20, bf16[]{:T(256)} %constant.58.clone.1), dimensions={0,2}, to_apply=%region_4.5 | reduce | flops 1179648 | bytes 3932162 | tf_op jit(solution)/shard_map/reduce_sum | solution.py:37
  157.6 2.5 copy.61
  160.1 11.5 %all-to-all-start.2 = ((bf16[64,1,12,512]{3,2,1,0:T(8,128)(2,1)}), bf16[64,1,12,512]{3,2,1,0:T(8,128)(2,1)}, u32[]{:S(2)}, u32[]{:S(2)}) async-start(bf16[64,1,12,512]{3,2,1,0:T(8,128)(2,1)} %copy.61), calls=%async_computation.2 | async-start | bytes 2097152 | tf_op jit(solution)/shard_map/all_to_all | solution.py:111
  171.7 3.5 %collective-permute-start.3 = (bf16[2,2,256]{2,1,0:T(2,128)(2,1)S(1)}, bf16[2,2,256]{2,1,0:T(2,128)(2,1)S(1)}, u32[]{:S(2)}, u32[]{:S(2)}) collective-permute-start(bf16[2,2,256]{2,1,0:T(2,128)(2,1)S(1)} %pad_maximum_fusion.2), channel_id=1, source_target_pairs={{0,4},{4,8},{8,12},{12,16},{16,20},{20,24},{24,28},{28,32},{32,36}... | collective-permute-start | bytes 6152 | tf_op jit(solution)/shard_map/ppermute | solution.py:43
  177.6 22.2 %all-to-all-done.2 = bf16[64,1,12,512]{3,2,1,0:T(8,128)(2,1)} async-done(((bf16[64,1,12,512]{3,2,1,0:T(8,128)(2,1)}), bf16[64,1,12,512]{3,2,1,0:T(8,128)(2,1)}, u32[]{:S(2)}, u32[]{:S(2)}) %all-to-all-start.2) | async-done | bytes 786464 | tf_op jit(solution)/shard_map/all_to_all | solution.py:111
  201.8 3.3 %gather_fusion = bf16[384,512]{1,0:T(8,128)(2,1)S(1)} fusion(bf16[768,512]{1,0:T(8,128)(2,1)} %reshape.172, s32[1024]{0:T(1024)S(1)} %pad_clamp_fusion), kind=kCustom, calls=%fused_computation | custom fusion | bytes 787968 | tf_op jit(solution)/shard_map/jit(_take)/gather | solution.py:116
  209.3 11.0 %all_gather.3 = bf16[192,2048]{1,0:T(8,128)(2,1)S(1)} all-gather(bf16[192,512]{1,0:T(8,128)(2,1)S(1)} %add_convert_fusion.1), channel_id=1, replica_groups=mesh['sp'=64,'tp'=4] {'tp'}, dimensions={1}, use_global_device_ids=true | all-gather | bytes 983040 | tf_op jit(solution)/shard_map/all_gather | solution.py:123
  220.2 2.5 multiply_convert_fusion.6
  224.2 9.6 %all-to-all-start.3 = ((bf16[64,32,256]{2,1,0:T(8,128)(2,1)}), bf16[64,32,256]{2,1,0:T(8,128)(2,1)}, u32[]{:S(2)}, u32[]{:S(2)}) async-start(bf16[64,32,256]{2,1,0:T(8,128)(2,1)} %bitcast.157), calls=%async_computation.3 | async-start | bytes 2097152 | tf_op jit(solution)/shard_map/all_to_all | solution.py:36
  233.8 3.1 %fusion.21 = bf16[1,2048,256]{1,2,0:T(8,128)(2,1)} fusion(bf16[64,1,12,2048]{3,0,2,1:T(8,128)(2,1)S(1)} %copy-done, bf16[64,1,12,256]{3,0,2,1:T(8,128)(2,1)} %copy-done.13), kind=kOutput, calls=%fused_computation.20 | convolution fusion | flops 805830656 | bytes 4587520 | tf_op jit(solution)/shard_map/secd,secf->edf/dot_general | solution.py:98
  239.6 2.4 collective-permute-start.4
  244.0 2.3 copy.62
  250.0 11.9 %all-to-all-done.3 = bf16[64,32,256]{2,1,0:T(8,128)(2,1)} async-done(((bf16[64,32,256]{2,1,0:T(8,128)(2,1)}), bf16[64,32,256]{2,1,0:T(8,128)(2,1)}, u32[]{:S(2)}, u32[]{:S(2)}) %all-to-all-start.3) | async-done | bytes 1048608 | tf_op jit(solution)/shard_map/all_to_all | solution.py:36
  (99 shorter events, 40.4 us)
Async XLA Ops:
  0.6 43.4 %copy-start = (bf16[64,1,12,2048]{3,0,2,1:T(8,128)(2,1)S(1)}, bf16[64,1,12,2048]{3,0,2,1:T(8,128)(2,1)}, u32[]{:S(2)}) copy-start(bf16[64,1,12,2048]{3,0,2,1:T(8,128)(2,1)} %param.15) | copy-start | bytes 9437188
  8.6 5.3 %copy-start.17 = (f32[192,2]{0,1:T(2,128)S(1)}, f32[192,2]{0,1:T(2,128)}, u32[]{:S(2)}) copy-start(f32[192,2]{0,1:T(2,128)} %param.14) | copy-start | bytes 4612
  30.7 41.4 %all-to-all-start = ((bf16[64,1,3,2048]{3,2,1,0:T(4,128)(2,1)}), bf16[64,1,3,2048]{3,2,1,0:T(4,128)(2,1)}, u32[]{:S(2)}, u32[]{:S(2)}) async-start(bf16[64,1,3,2048]{3,2,1,0:T(4,128)(2,1)} %dynamic-slice_bitcast_fusion), calls=%async_computation | async-start | bytes 2097152 | tf_op jit(solution)/shard_map/all_to_all | solution.py:84
  73.9 19.2 %collective-permute-start = (bf16[64,1,3,2048]{3,0,2,1:T(8,128)(2,1)S(1)}, bf16[64,1,3,2048]{3,0,2,1:T(8,128)(2,1)S(1)}, u32[]{:S(2)}, u32[]{:S(2)}) collective-permute-start(bf16[64,1,3,2048]{3,0,2,1:T(8,128)(2,1)S(1)} %copy.55), channel_id=1, source_target_pairs={{0,1},{1,2},{2,3},{3,0},{4,5},{5,6},{6,7},{7,4},{8,9},{9,10},{10,1... | collective-permute-start | bytes 2359304 | tf_op jit(solution)/shard_map/ppermute | solution.py:16
  77.4 34.1 %copy-start.21 = (f32[64,1,12,256]{3,0,2,1:T(8,128)}, f32[64,1,12,256]{3,0,2,1:T(8,128)S(1)}, u32[]{:S(2)}) copy-start(f32[64,1,12,256]{3,0,2,1:T(8,128)S(1)} %fusion.31) | copy-start | bytes 2359300
  77.4 17.9 %collective-permute-start.1 = (bf16[64,1,3,2048]{3,0,2,1:T(8,128)(2,1)S(1)}, bf16[64,1,3,2048]{3,0,2,1:T(8,128)(2,1)S(1)}, u32[]{:S(2)}, u32[]{:S(2)}) collective-permute-start(bf16[64,1,3,2048]{3,0,2,1:T(8,128)(2,1)S(1)} %copy.55), channel_id=1, source_target_pairs={{0,3},{1,0},{2,1},{3,2},{4,7},{5,4},{6,5},{7,6},{8,11},{9,8},{10,9... | collective-permute-start | bytes 2359304 | tf_op jit(solution)/shard_map/ppermute | solution.py:21
  79.5 32.0 %copy-start.18 = (bf16[1,256,2048]{2,1,0:T(8,128)(2,1)S(1)}, bf16[1,256,2048]{2,1,0:T(8,128)(2,1)}, u32[]{:S(2)}) copy-start(bf16[1,256,2048]{2,1,0:T(8,128)(2,1)} %param.18) | copy-start | bytes 3145732
  79.5 32.0 %copy-start.19 = (f32[64,1,12,256]{3,0,2,1:T(8,128)S(1)}, f32[64,1,12,256]{3,0,2,1:T(8,128)}, u32[]{:S(2)}) copy-start(f32[64,1,12,256]{3,0,2,1:T(8,128)} %fusion.34) | copy-start | bytes 2359300
  93.1 18.3 %collective-permute-start.2 = (bf16[64,1,3,2048]{3,0,2,1:T(8,128)(2,1)S(1)}, bf16[64,1,3,2048]{3,0,2,1:T(8,128)(2,1)S(1)}, u32[]{:S(2)}, u32[]{:S(2)}) collective-permute-start(bf16[64,1,3,2048]{3,0,2,1:T(8,128)(2,1)S(1)} %collective-permute-done), channel_id=1, source_target_pairs={{0,1},{1,2},{2,3},{3,0},{4,5},{5,6},{6,7},{7,4},{8,9},{9,10},{10,1... | collective-permute-start | bytes 2359304 | tf_op jit(solution)/shard_map/ppermute | solution.py:16
  154.1 17.6 %copy-start.6 = (bf16[192,256]{1,0:T(8,128)(2,1)S(1)}, bf16[192,256]{1,0:T(8,128)(2,1)}, u32[]{:S(2)}) copy-start(bf16[192,256]{1,0:T(8,128)(2,1)} %param.19) | copy-start | bytes 294916
  154.1 17.6 %copy-start.8 = (bf16[192,256]{1,0:T(8,128)(2,1)S(1)}, bf16[192,256]{1,0:T(8,128)(2,1)}, u32[]{:S(2)}) copy-start(bf16[192,256]{1,0:T(8,128)(2,1)} %param.21) | copy-start | bytes 294916
  154.1 21.5 %copy-start.14 = (s32[192,2]{0,1:T(2,128)S(1)}, s32[192,2]{0,1:T(2,128)}, u32[]{:S(2)}) copy-start(s32[192,2]{0,1:T(2,128)} %param.13) | copy-start | bytes 4612
  154.1 21.5 %copy-start.16 = (f32[3,256]{1,0:T(4,128)S(1)}, f32[3,256]{1,0:T(4,128)}, u32[]{:S(2)}) copy-start(f32[3,256]{1,0:T(4,128)} %param.22) | copy-start | bytes 9220
  160.1 39.6 %all-to-all-start.2 = ((bf16[64,1,12,512]{3,2,1,0:T(8,128)(2,1)}), bf16[64,1,12,512]{3,2,1,0:T(8,128)(2,1)}, u32[]{:S(2)}, u32[]{:S(2)}) async-start(bf16[64,1,12,512]{3,2,1,0:T(8,128)(2,1)} %copy.61), calls=%async_computation.2 | async-start | bytes 2097152 | tf_op jit(solution)/shard_map/all_to_all | solution.py:111
  171.7 5.3 %collective-permute-start.3 = (bf16[2,2,256]{2,1,0:T(2,128)(2,1)S(1)}, bf16[2,2,256]{2,1,0:T(2,128)(2,1)S(1)}, u32[]{:S(2)}, u32[]{:S(2)}) collective-permute-start(bf16[2,2,256]{2,1,0:T(2,128)(2,1)S(1)} %pad_maximum_fusion.2), channel_id=1, source_target_pairs={{0,4},{4,8},{8,12},{12,16},{16,20},{20,24},{24,28},{28,32},{32,36}... | collective-permute-start | bytes 6152 | tf_op jit(solution)/shard_map/ppermute | solution.py:43
  205.2 15.1 %copy-start.15 = (f32[2,256]{1,0:T(2,128)S(1)}, f32[2,256]{1,0:T(2,128)}, u32[]{:S(2)}) copy-start(f32[2,256]{1,0:T(2,128)} %multiply_bitcast_fusion) | copy-start | bytes 6148
  206.1 16.6 %copy-start.10 = (bf16[192,256]{1,0:T(8,128)(2,1)S(1)}, bf16[192,256]{1,0:T(8,128)(2,1)}, u32[]{:S(2)}) copy-start(bf16[192,256]{1,0:T(8,128)(2,1)} %param.20) | copy-start | bytes 294916
  209.3 14.9 %copy-start.5 = (bf16[192,512]{1,0:T(8,128)(2,1)}, bf16[192,512]{1,0:T(8,128)(2,1)S(1)}, u32[]{:S(2)}) copy-start(bf16[192,512]{1,0:T(8,128)(2,1)S(1)} %add_convert_fusion.1) | copy-start | bytes 589828
  224.2 37.7 %all-to-all-start.3 = ((bf16[64,32,256]{2,1,0:T(8,128)(2,1)}), bf16[64,32,256]{2,1,0:T(8,128)(2,1)}, u32[]{:S(2)}, u32[]{:S(2)}) async-start(bf16[64,32,256]{2,1,0:T(8,128)(2,1)} %bitcast.157), calls=%async_computation.3 | async-start | bytes 2097152 | tf_op jit(solution)/shard_map/all_to_all | solution.py:36
  233.8 3.2 %copy-start.2 = (bf16[64,12,2048]{2,0,1:T(8,128)(2,1)S(1)}, bf16[64,12,2048]{2,0,1:T(8,128)(2,1)}, u32[]{:S(2)}) copy-start(bf16[64,12,2048]{2,0,1:T(8,128)(2,1)} %copy-done.1) | copy-start | bytes 9437188
  237.0 5.1 %copy-start.12 = (bf16[64,1,12,256]{3,0,2,1:T(8,128)(2,1)S(1)}, bf16[64,1,12,256]{3,0,2,1:T(8,128)(2,1)}, u32[]{:S(2)}) copy-start(bf16[64,1,12,256]{3,0,2,1:T(8,128)(2,1)} %copy-done.11) | copy-start | bytes 1179652
  239.6 9.0 %collective-permute-start.4 = (f32[2,256]{1,0:T(2,128)}, f32[2,256]{1,0:T(2,128)S(1)}, u32[]{:S(2)}, u32[]{:S(2)}) collective-permute-start(f32[2,256]{1,0:T(2,128)} %slice.66), channel_id=1, source_target_pairs={{4,0},{8,4},{12,8},{16,12},{20,16},{24,20},{28,24},{32,28},{36,32}... | collective-permute-start | bytes 6152 | tf_op jit(solution)/shard_map/ppermute | solution.py:43
  244.0 4.6 %copy-start.7 = (bf16[192,256]{1,0:T(8,128)(2,1)S(1)}, bf16[192,256]{1,0:T(8,128)(2,1)}, u32[]{:S(2)}) copy-start(bf16[192,256]{1,0:T(8,128)(2,1)} %param.19) | copy-start | bytes 294916
  244.0 5.3 %copy-start.9 = (bf16[192,256]{1,0:T(8,128)(2,1)S(1)}, bf16[192,256]{1,0:T(8,128)(2,1)}, u32[]{:S(2)}) copy-start(bf16[192,256]{1,0:T(8,128)(2,1)} %param.21) | copy-start | bytes 294916
  (7 other events, 14.0 us)
